TPU v7x, 256 devices: a whole 4x4x8 slice. The times are simulated.
256 devices in a mesh: ep: 64 (over z, y, core), tp: 4 (over x).
Axes of the slice: x: 4, y: 4, z: 8, core: 2. Of those that a mesh axis runs over, the one named last changes fastest.
Arguments:
- state_probe_logits: bfloat16 [65536, 1024], P('ep', 'tp'), may hold values from -6 to 6
- retention_logits: bfloat16 [65536, 1024], P('ep', 'tp'), may hold values from -12 to 12
- state_source_entries: bfloat16 [65536, 1024], P('ep', 'tp'), may hold values from -6 to 6
- state_result_switch_logits: bfloat16 [65536, 1024], P('ep', 'tp'), may hold values from -6 to 6
- retention_bound_margin: float32 [1024], P('tp'), may hold values from 0 to 0.07
- extra_fading_amount: float32 [65536, 8], P('ep', 'tp'), may hold values from -0.7 to 0
- state_result_scale: float32 [1024], P('tp'), may hold values from 0.1 to 1.9
- state_result_matrix: bfloat16 [1024, 2048], P(None, 'tp'), may hold values from -0.1875 to 0.1875
- second_slice_tokens: bfloat16 [32768, 2048], P('ep'), may hold values from -6 to 6
- specialist_assignment: int32 [32768, 2], P('ep'), may hold values from 0 to 63, all different within a row; in each aligned block of 128 rows (0 to 127, 128 to 255, ...) at most 8 rows name the same one
- selected_specialist_share: float32 [32768, 2], P('ep'), may hold values from 0.1 to 1
- leading_scale_vector: float32 [2048], replicated, may hold values from 0.1 to 1.9
- trailing_scale_vector: float32 [2048], replicated, may hold values from 0.1 to 1.9
- specialist_switch_matrix: bfloat16 [64, 2048, 2048], P('ep', None, 'tp'), may hold values from -0.3125 to 0.3125
- specialist_widen_matrix: bfloat16 [64, 2048, 2048], P('ep', None, 'tp'), may hold values from -0.3125 to 0.3125
- specialist_contract_matrix: bfloat16 [64, 2048, 2048], P('ep', 'tp'), may hold values from -0.125 to 0.125
Outputs:
- mixer_out: bfloat16 [65536, 2048], P('ep', 'tp')
- moe_out: bfloat16 [32768, 2048], P(('ep', 'tp'))
Inputs may be any that keep to these rules, and one draw needn't show every extreme that they name: `specialist_assignment`: each row names 2 different experts. In each aligned block of 128 rows no expert is named by more than 8 rows, a bound that some block reaches.
All inputs are finite; a program needn't handle non-finite values.
Results may differ from a plain program's by a relative error of at most 0.012.
Values may be sent and summed in bfloat16 or wider, within the bound.
No kernel may reach another device: no remote copies, remote signals or barrier semaphores. Data moves between devices by JAX's collectives and lax.ppermute only.
A program may use at most 128 MiB of HBM per device.

v0:
```python
import jax
import jax.numpy as jnp
from jax import lax
from jax.sharding import Mesh
from jax.sharding import PartitionSpec as P

HEAD = 128
SPAN_STEPS = 64
TOK_DEV = 128
EP = ("ep_0", "ep_1", "ep_2")
EP_TP = ("ep_0", "ep_1", "ep_2", "tp")
NORM_EPS = 1e-06
SWISH_ALPHA = 1.702
CLAMP_LIMIT = 7.0


def sent_to_all(shard, axis):
    length = lax.axis_size(axis)
    return lax.all_to_all(
        jnp.broadcast_to(shard[None], (length, *shard.shape)), axis, 0, 0, tiled=True
    )


def joined_along(tiles, dim):
    shape = list(tiles.shape[1:])
    shape[dim] *= tiles.shape[0]
    return jnp.moveaxis(tiles, 0, dim).reshape(shape)


def gathered_copies(shard, axis, dim):
    tiles = sent_to_all(shard, axis)
    return joined_along(tiles, dim)


def all_blocks(shard, axes, order):
    tiles = shard[None]
    for k in order:
        tiles = lax.all_gather(tiles, axes[k], axis=0, tiled=True)
    current = [lax.axis_size(axes[k]) for k in reversed(order)]
    tiles = tiles.reshape(*current, *shard.shape)
    turned = sorted(range(len(order)), key=lambda place: order[len(order) - 1 - place])
    return tiles.transpose(*turned, *range(len(order), tiles.ndim)).reshape(-1, *shard.shape)


def gather_axes(shard, axes, order, dim):
    return joined_along(all_blocks(shard, axes, order), dim)


def in_blocks(shard, dim, length):
    before, after = (shard.shape[:dim], shard.shape[dim + 1 :])
    return jnp.moveaxis(shard.reshape(*before, length, -1, *after), dim, 0)


def sum_at_owner(shard, axis, dim):
    length = lax.axis_size(axis)
    tiles = lax.all_to_all(in_blocks(shard, dim, length), axis, 0, 0, tiled=True)
    return jnp.sum(tiles.astype(jnp.float32), axis=0)


def rms_scale(values, gain):
    return values * lax.rsqrt(jnp.mean(values * values, axis=-1, keepdims=True) + NORM_EPS) * gain


def clamped_unit(gate, upward):
    glued = jnp.minimum(gate, CLAMP_LIMIT)
    linear = jnp.clip(upward, -CLAMP_LIMIT, CLAMP_LIMIT)
    return glued * jax.nn.sigmoid(SWISH_ALPHA * glued) * (linear + 1.0)


def slot_table(routes, quarters, experts, capacity):
    per_quarter = routes.shape[0] * routes.shape[1] // quarters
    flat = routes.reshape(quarters, per_quarter)
    onehot = (flat[:, :, None] == jnp.arange(experts, dtype=jnp.int32)[None, None, :]).astype(
        jnp.int32
    )
    rank = jnp.sum(onehot * (jnp.cumsum(onehot, axis=1) - 1), axis=2)
    quarter_ids = jnp.arange(quarters, dtype=jnp.int32)[:, None]
    return ((quarter_ids * experts + flat) * capacity + rank).reshape(-1)


def pack_rows(normed, routes, quarters, experts, capacity):
    slots = slot_table(routes, quarters, experts, capacity)
    room = quarters * experts * capacity
    owner = jnp.arange(slots.shape[0], dtype=jnp.int32) // routes.shape[1]
    source = jnp.zeros((room,), jnp.int32).at[slots].set(owner)
    filled = jnp.zeros((room,), jnp.bool_).at[slots].set(True)
    packed = jnp.where(filled[:, None], normed[source], jnp.zeros((), jnp.bfloat16))
    return packed.reshape(quarters, experts, capacity, normed.shape[1])


def shards(
    state_probe_logits,
    retention_logits,
    state_source_entries,
    state_result_switch_logits,
    retention_bound_margin,
    extra_fading_amount,
    state_result_scale,
    state_result_matrix,
    second_slice_tokens,
    specialist_assignment,
    selected_specialist_share,
    leading_scale_vector,
    trailing_scale_vector,
    specialist_switch_matrix,
    specialist_widen_matrix,
    specialist_contract_matrix,
):
    total_rows, width = state_probe_logits.shape
    groups_each_device = width // HEAD
    span_tally = total_rows // SPAN_STEPS

    def per_head(values):
        return values.reshape(span_tally, SPAN_STEPS, groups_each_device, HEAD).transpose(
            0, 2, 1, 3
        )

    query = per_head(jax.nn.silu(state_probe_logits.astype(jnp.float32)) * HEAD ** (-0.5))
    input_key = per_head(
        retention_bound_margin * jax.nn.sigmoid(-retention_logits.astype(jnp.float32))
    )
    decay_logarithm = (
        jnp.log1p(-input_key)
        + extra_fading_amount.reshape(span_tally, SPAN_STEPS, groups_each_device).transpose(
            0, 2, 1
        )[..., None]
    )
    values = per_head(state_source_entries.astype(jnp.float32))
    cumul = jnp.cumsum(decay_logarithm, axis=2)
    middle = cumul[:, :, SPAN_STEPS // 2 - 1 : SPAN_STEPS // 2]
    last = cumul[:, :, SPAN_STEPS - 1 :]
    causal = jnp.tril(jnp.ones((SPAN_STEPS, SPAN_STEPS), jnp.float32))
    scores = (
        jnp.einsum(
            "nhid,nhjd->nhij", query * jnp.exp(cumul - middle), input_key * jnp.exp(middle - cumul)
        )
        * causal
    )
    inner = jnp.einsum("nhij,nhje->nhie", scores, values)
    update = jnp.einsum("nhcd,nhce->nhde", input_key * jnp.exp(last - cumul), values)
    block_decay = last[:, :, 0]

    def advance(state, operand_tensors):
        decay_log, addition = operand_tensors
        return (jnp.exp(decay_log)[..., None] * state + addition, state)

    end_state, local_start = lax.scan(
        advance, jnp.zeros((groups_each_device, HEAD, HEAD), jnp.float32), (block_decay, update)
    )
    decay_total = jnp.sum(block_decay, axis=0)
    running = jnp.cumsum(block_decay, axis=0)
    before = jnp.concatenate([jnp.zeros_like(running[:1]), running[:-1]], axis=0)
    totals = gathered_copies(decay_total[None], EP, 0)
    through = jnp.cumsum(totals, axis=0)
    my_index = lax.axis_index(EP)
    reach = lax.dynamic_index_in_dim(through - totals, my_index, 0, keepdims=False)
    portion = gather_axes(end_state[None].astype(jnp.bfloat16), EP, (1, 0, 2), 0).astype(
        jnp.float32
    )
    length = portion.shape[0]
    earlier = jnp.arange(length, dtype=jnp.int32) < my_index
    weights = jnp.where(
        earlier[:, None, None], jnp.exp(jnp.minimum(reach[None] - through, 0.0)), 0.0
    )
    entering = jnp.zeros_like(end_state) + jnp.einsum("jhd,jhde->hde", weights, portion)
    start_state = local_start + jnp.exp(before)[..., None] * entering[None]
    outer = jnp.einsum("nhcd,nhde->nhce", query * jnp.exp(cumul), start_state)
    raw_out = inner + outer
    normed_rec = raw_out * lax.rsqrt(jnp.mean(raw_out * raw_out, axis=-1, keepdims=True) + NORM_EPS)
    normed_rec = normed_rec.transpose(0, 2, 1, 3).reshape(total_rows, width)
    state_layer_result = (
        normed_rec
        * state_result_scale
        * jax.nn.silu(state_result_switch_logits.astype(jnp.float32))
    ).astype(jnp.bfloat16)
    mixed = jnp.dot(
        lax.all_gather(state_layer_result, "tp", axis=1, tiled=True),
        state_result_matrix,
        preferred_element_type=jnp.float32,
    )
    mixer_out = mixed.astype(jnp.bfloat16)
    experts = specialist_switch_matrix.shape[0] * lax.axis_size(EP)
    top_count = specialist_assignment.shape[1]
    capacity = 2 * TOK_DEV * top_count // experts
    my_quarter = lax.axis_index("tp")
    own_route = lax.dynamic_slice_in_dim(specialist_assignment, my_quarter * TOK_DEV, TOK_DEV, 0)
    own_weight = lax.dynamic_slice_in_dim(
        selected_specialist_share, my_quarter * TOK_DEV, TOK_DEV, 0
    )
    own_rows = lax.dynamic_slice_in_dim(second_slice_tokens, my_quarter * TOK_DEV, TOK_DEV, 0)
    normed = rms_scale(own_rows.astype(jnp.float32), leading_scale_vector).astype(jnp.bfloat16)
    packed = pack_rows(normed, own_route, 1, experts, capacity)[0]
    arrived = lax.all_to_all(packed, EP, split_axis=0, concat_axis=0, tiled=True)
    portion = lax.all_gather(arrived.reshape(-1, arrived.shape[2]), "tp", axis=0, tiled=True)
    gate = jnp.dot(portion, specialist_switch_matrix[0], preferred_element_type=jnp.float32)
    upward = jnp.dot(portion, specialist_widen_matrix[0], preferred_element_type=jnp.float32)
    activated = clamped_unit(gate, upward).astype(jnp.bfloat16)
    summed = sum_at_owner(
        jnp.dot(
            activated, specialist_contract_matrix[0], preferred_element_type=jnp.float32
        ).astype(jnp.bfloat16),
        "tp",
        0,
    )
    finished = summed.astype(jnp.bfloat16).reshape(-1, capacity, summed.shape[1])
    returned = lax.all_to_all(finished, EP, split_axis=0, concat_axis=0, tiled=True)
    flat_back = returned.reshape(-1, returned.shape[2])
    own_slots = slot_table(own_route, 1, experts, capacity).reshape(TOK_DEV, top_count)
    combined = jnp.zeros((TOK_DEV, flat_back.shape[1]), jnp.float32)
    for column in range(top_count):
        combined = (
            combined
            + flat_back[own_slots[:, column]].astype(jnp.float32)
            * own_weight[:, column : column + 1]
        )
    moe_out = rms_scale(combined, trailing_scale_vector).astype(jnp.bfloat16)
    return (mixer_out, moe_out)


def solution(mesh):
    finer = Mesh(mesh.devices.reshape(8, 4, 2, mesh.shape["tp"]), ("ep_0", "ep_1", "ep_2", "tp"))
    placed = (
        P(EP, "tp"),
        P(EP, "tp"),
        P(EP, "tp"),
        P(EP, "tp"),
        P("tp"),
        P(EP, "tp"),
        P("tp"),
        P(None, "tp"),
        P(EP, None),
        P(EP, None),
        P(EP, None),
        P(),
        P(),
        P(EP, None, "tp"),
        P(EP, None, "tp"),
        P(EP, "tp", None),
    )
    return jax.shard_map(
        shards,
        mesh=finer,
        in_specs=placed,
        out_specs=(P(EP, "tp"), P(EP_TP, None)),
        check_vma=False,
    )
```

profile of v0, /device:TPU:8, one launch (start us, length us, event | category | flops | bytes accessed | tf_op | source)
XLA Modules:
  0.0 367.5 jit_solution(13056595619154716890)
XLA Ops:
  10.0 1.4 scatter_custom_fusion.1
  11.4 1.2 fusion.17
  12.7 1.5 scatter_custom_fusion
  14.3 1.3 fusion.19
  15.5 3.3 gather_fusion
  18.9 1.8 bitcast_select_fusion
  20.7 63.2 %all_to_all.20 = bf16[64,8,2048]{2,1,0:T(8,128)(2,1)} all-to-all(bf16[64,8,2048]{2,1,0:T(8,128)(2,1)S(1)} %bitcast_select_fusion), channel_id=1, replica_groups=mesh['ep_0'=8,'ep_1'=4,'ep_2'=2,'tp'=4] {'ep_0','ep_1','ep_2'}, dimensions={0} | all-to-all | bytes 4194304 | tf_op jit(solution)/shard_map/all_to_all | solution.py:193
  85.0 1.3 divide_multiply_fusion
  86.2 1.7 reshape.256
  90.6 5.4 %all-to-all-start = ((f32[64,1,2,128]{3,2,1,0:T(2,128)}), f32[64,1,2,128]{3,2,1,0:T(2,128)S(1)}, u32[]{:S(2)}, u32[]{:S(2)}) async-start(f32[64,1,2,128]{3,2,1,0:T(2,128)} %broadcast_in_dim.86), calls=%async_computation | async-start | bytes 131072 | tf_op jit(solution)/shard_map/all_to_all | solution.py:19
  96.1 2.3 fusion.12
  98.5 2.7 reshape.255
  101.2 2.0 reshape.258
  103.2 4.3 %bitcast_multiply_fusion.5 = (bf16[16,2,64,128]{3,0,1,2:T(8,128)(2,1)}, bf16[16,2,64,128]{3,0,1,2:T(8,128)(2,1)}, bf16[16,2,64,128]{3,0,1,2:T(8,128)(2,1)S(1)}, bf16[16,2,64,128]{3,0,1,2:T(8,128)(2,1)}) fusion(f32[16,2,64,128]{3,0,1,2:T(8,128)} %copy-done.5, f32[16,64,2,128]{3,2,1,0:T(2,128)} %reshape.255, f32[16,2,128]{2,0,1:T(8,128)S(1)} %get-tuple-element.88, ...), kind=kLoop, calls=%fused_computation.49 | loop fusion | flops 2883584 | bytes 5275648 | tf_op jit(solution)/shard_map/mul | solution.py:135
  107.5 1.8 fusion.25
  109.3 27.5 %while.13 = (s32[]{:T(128)}, f32[2,128,128]{2,1,0:T(8,128)S(1)}, f32[16,2,128,128]{3,2,1,0:T(8,128)}, f32[16,2,128]{2,1,0:T(2,128)S(1)}, f32[16,2,128,128]{3,2,1,0:T(8,128)}, /*index=5*/s32[]{:T(128)}, s32[]{:T(128)}) while((s32[]{:T(128)}, f32[2,128,128]{2,1,0:T(8,128)S(1)}, f32[16,2,128,128]{3,2,1,0:T(8,128)}, ...), condition=%wide.region_2.3_spmd.clone, body=%wide.region_1.2_spmd.clone.sunk | while | flops 131075 | bytes 659040 | solution.py:147
  109.9 1.0 bitcast_add_fusion.2
  111.6 1.0 bitcast_add_fusion.2
  113.4 1.0 bitcast_add_fusion.2
  116.8 1.0 bitcast_add_fusion.2
  118.5 1.0 bitcast_add_fusion.2
  122.0 1.0 bitcast_add_fusion.2
  123.7 1.0 bitcast_add_fusion.2
  127.1 1.0 bitcast_add_fusion.2
  128.9 1.0 bitcast_add_fusion.2
  134.0 1.0 bitcast_add_fusion.2
  135.7 1.0 bitcast_add_fusion.2
  136.8 13.2 %all-gather = bf16[8,128,128]{2,1,0:T(8,128)(2,1)} all-gather(bf16[2,128,128]{2,1,0:T(8,128)(2,1)S(1)} %convert_element_type.56), channel_id=2, replica_groups=mesh['ep_0'=8,'ep_1'=4,'ep_2'=2,'tp'=4] {'ep_1'}, dimensions={0}, use_global_device_ids=true | all-gather | bytes 327680 | tf_op jit(solution)/shard_map/all_gather | solution.py:38
  150.0 15.9 %all-gather.12.cloned.1.call-done = bf16[2048,2048]{1,0:T(8,128)(2,1)} async-done(((bf16[512,2048]{1,0:T(8,128)(2,1)}), bf16[2048,2048]{1,0:T(8,128)(2,1)}) %all-gather.12.cloned.1.call-update) | async-done | bytes 8388624 | tf_op jit(solution)/shard_map/all_gather | solution.py:194
  165.9 7.7 %fusion.4 = f32[2048,512]{1,0:T(8,128)S(1)} fusion(bf16[2048,2048]{1,0:T(8,128)(2,1)} %all-gather.12.cloned.1.call-done, bf16[1,2048,512]{2,1,0:T(8,128)(2,1)} %param.31), kind=kOutput, calls=%fused_computation.14 | convolution fusion | flops 4294967296 | bytes 14680064 | tf_op jit(solution)/shard_map/dot_general | solution.py:195
  173.6 5.6 %multiply_convert_fusion = bf16[2048,512]{1,0:T(8,128)(2,1)S(1)} fusion(f32[2048,512]{1,0:T(8,128)S(1)} %fusion.4, bf16[2048,2048]{1,0:T(8,128)(2,1)S(1)} %copy-done.15, bf16[1,2048,512]{2,1,0:T(8,128)(2,1)S(1)} %copy-done.16), kind=kOutput, calls=%fused_computation.11 | convolution fusion | flops 4305453056 | bytes 16777216 | tf_op jit(solution)/shard_map/dot_general | solution.py:196
  179.2 6.7 %convolution_convert_fusion = bf16[2048,2048]{1,0:T(8,128)(2,1)} fusion(bf16[2048,512]{1,0:T(8,128)(2,1)S(1)} %multiply_convert_fusion, bf16[1,512,2048]{2,1,0:T(8,128)(2,1)S(1)} %copy-done), kind=kOutput, calls=%fused_computation.8 | convolution fusion | flops 4299161600 | bytes 12582912 | tf_op jit(solution)/shard_map/dot_general | solution.py:199
  186.0 5.7 %all-to-all-start.2 = ((bf16[4,512,2048]{2,1,0:T(8,128)(2,1)}), bf16[4,512,2048]{2,1,0:T(8,128)(2,1)}, u32[]{:S(2)}, u32[]{:S(2)}) async-start(bf16[4,512,2048]{2,1,0:T(8,128)(2,1)} %bitcast.107), calls=%async_computation.2 | async-start | bytes 16777216 | tf_op jit(solution)/shard_map/all_to_all | solution.py:56
  191.7 17.9 %all-gather.6.cloned.1.call-done = bf16[32,1,2,128,128]{4,3,2,1,0:T(8,128)(2,1)} async-done(((bf16[4,1,2,128,128]{4,3,2,1,0:T(8,128)(2,1)}), bf16[32,1,2,128,128]{4,3,2,1,0:T(8,128)(2,1)}) %all-gather.6.cloned.1.call-update) | async-done | bytes 2097168 | tf_op jit(solution)/shard_map/all_gather | solution.py:38
  210.0 18.9 %all-gather.8.cloned.1.call-done = bf16[64,1,2,128,128]{4,3,2,1,0:T(8,128)(2,1)} async-done(((bf16[32,1,2,128,128]{4,3,2,1,0:T(8,128)(2,1)}), bf16[64,1,2,128,128]{4,3,2,1,0:T(8,128)(2,1)}) %all-gather.8.cloned.1.call-update) | async-done | bytes 4194320 | tf_op jit(solution)/shard_map/all_gather | solution.py:38
  229.0 2.5 copy.63
  231.5 2.8 fusion
  234.3 1.1 fusion.6
  235.5 1.9 multiply_reduce_fusion.1
  237.4 48.2 %all-to-all-done.2 = bf16[4,512,2048]{2,1,0:T(8,128)(2,1)} async-done(((bf16[4,512,2048]{2,1,0:T(8,128)(2,1)}), bf16[4,512,2048]{2,1,0:T(8,128)(2,1)}, u32[]{:S(2)}, u32[]{:S(2)}) %all-to-all-start.2) | async-done | bytes 8388640 | tf_op jit(solution)/shard_map/all_to_all | solution.py:56
  285.6 7.3 %reduce_sum.70 = bf16[512,2048]{1,0:T(8,128)(2,1)} reduce(bf16[4,512,2048]{2,1,0:T(8,128)(2,1)} %all-to-all-done.2, bf16[]{:T(256)} %constant.117.clone.1), dimensions={0}, to_apply=%region_13.14 | reduce | flops 3145728 | bytes 10485762 | tf_op jit(solution)/shard_map/reduce_sum | solution.py:57
  292.8 10.6 %all-to-all-start.3 = ((bf16[64,8,2048]{2,1,0:T(8,128)(2,1)}), bf16[64,8,2048]{2,1,0:T(8,128)(2,1)S(1)}, u32[]{:S(2)}, u32[]{:S(2)}) async-start(bf16[64,8,2048]{2,1,0:T(8,128)(2,1)} %bitcast.109), calls=%async_computation.3 | async-start | bytes 4194304 | tf_op jit(solution)/shard_map/all_to_all | solution.py:206
  304.9 1.1 fusion.33
  306.9 35.1 %all-gather.10.cloned.1.call-done = bf16[1024,1024]{1,0:T(8,128)(2,1)} async-done(((bf16[1024,256]{1,0:T(8,128)(2,1)}), bf16[1024,1024]{1,0:T(8,128)(2,1)}) %all-gather.10.cloned.1.call-update) | async-done | bytes 2097168 | tf_op jit(solution)/shard_map/all_gather | solution.py:177
  342.0 4.1 %convolution_convert_fusion.1 = bf16[1024,512]{1,0:T(8,128)(2,1)} fusion(bf16[1024,1024]{1,0:T(8,128)(2,1)} %all-gather.10.cloned.1.call-done, bf16[1024,512]{1,0:T(8,128)(2,1)} %param.25), kind=kOutput, calls=%fused_computation.20 | convolution fusion | flops 1074266112 | bytes 4194304 | tf_op jit(solution)/shard_map/dot_general | solution.py:176
  346.1 8.6 %all-to-all-done.3 = bf16[64,8,2048]{2,1,0:T(8,128)(2,1)S(1)} async-done(((bf16[64,8,2048]{2,1,0:T(8,128)(2,1)}), bf16[64,8,2048]{2,1,0:T(8,128)(2,1)S(1)}, u32[]{:S(2)}, u32[]{:S(2)}) %all-to-all-start.3) | async-done | bytes 2097184 | tf_op jit(solution)/shard_map/all_to_all | solution.py:206
  356.0 3.5 gather_fusion.2
  359.9 1.1 multiply_convert_fusion.1
  (131 shorter events, 27.0 us)
Async XLA Ops:
  7.2 172.1 %copy-start = (bf16[1,512,2048]{2,1,0:T(8,128)(2,1)S(1)}, bf16[1,512,2048]{2,1,0:T(8,128)(2,1)}, u32[]{:S(2)}) copy-start(bf16[1,512,2048]{2,1,0:T(8,128)(2,1)} %param.33) | copy-start | bytes 6291460
  7.2 158.7 %all-gather.12.cloned.1.call-start = ((), (), s32[]{:S(2)}) async-start(), calls=%async_computation.7 | async-start | bytes 10485760 | tf_op jit(solution)/shard_map/all_gather | solution.py:194
  83.9 1.0 copy-start.9
  83.9 1.0 copy-start.14
  85.0 3.0 copy-start.12
  89.0 1.0 copy-start.5
  90.6 95.4 %all-to-all-start = ((f32[64,1,2,128]{3,2,1,0:T(2,128)}), f32[64,1,2,128]{3,2,1,0:T(2,128)S(1)}, u32[]{:S(2)}, u32[]{:S(2)}) async-start(f32[64,1,2,128]{3,2,1,0:T(2,128)} %broadcast_in_dim.86), calls=%async_computation | async-start | bytes 131072 | tf_op jit(solution)/shard_map/all_to_all | solution.py:19
  96.0 113.5 %all-gather.6.cloned.1.call-start = ((), (), s32[]{:S(2)}) async-start(), calls=%async_computation.4 | async-start | bytes 2359296 | tf_op jit(solution)/shard_map/all_gather | solution.py:38
  103.2 4.3 %copy-start.3 = (bf16[16,64,2,128]{3,2,1,0:T(2,128)(2,1)S(1)}, bf16[16,64,2,128]{3,2,1,0:T(2,128)(2,1)}, u32[]{:S(2)}) copy-start(bf16[16,64,2,128]{3,2,1,0:T(2,128)(2,1)} %reshape.258) | copy-start | bytes 1572868
  165.9 7.7 %copy-start.15 = (bf16[2048,2048]{1,0:T(8,128)(2,1)S(1)}, bf16[2048,2048]{1,0:T(8,128)(2,1)}, u32[]{:S(2)}) copy-start(bf16[2048,2048]{1,0:T(8,128)(2,1)} %all-gather.12.cloned.1.call-done) | copy-start | bytes 25165828
  165.9 7.7 %copy-start.16 = (bf16[1,2048,512]{2,1,0:T(8,128)(2,1)S(1)}, bf16[1,2048,512]{2,1,0:T(8,128)(2,1)}, u32[]{:S(2)}) copy-start(bf16[1,2048,512]{2,1,0:T(8,128)(2,1)} %param.32) | copy-start | bytes 6291460
  186.0 99.6 %all-to-all-start.2 = ((bf16[4,512,2048]{2,1,0:T(8,128)(2,1)}), bf16[4,512,2048]{2,1,0:T(8,128)(2,1)}, u32[]{:S(2)}, u32[]{:S(2)}) async-start(bf16[4,512,2048]{2,1,0:T(8,128)(2,1)} %bitcast.107), calls=%async_computation.2 | async-start | bytes 16777216 | tf_op jit(solution)/shard_map/all_to_all | solution.py:56
  191.6 37.3 %all-gather.8.cloned.1.call-start = ((), (), s32[]{:S(2)}) async-start(), calls=%async_computation.5 | async-start | bytes 6291456 | tf_op jit(solution)/shard_map/all_gather | solution.py:38
  231.5 2.9 copy-start.7
  231.5 2.9 copy-start.8
  234.3 1.1 copy-start.4
  234.3 1.2 copy-start.6
  292.8 61.8 %all-to-all-start.3 = ((bf16[64,8,2048]{2,1,0:T(8,128)(2,1)}), bf16[64,8,2048]{2,1,0:T(8,128)(2,1)S(1)}, u32[]{:S(2)}, u32[]{:S(2)}) async-start(bf16[64,8,2048]{2,1,0:T(8,128)(2,1)} %bitcast.109), calls=%async_computation.3 | async-start | bytes 4194304 | tf_op jit(solution)/shard_map/all_to_all | solution.py:206
  303.4 38.6 %all-gather.10.cloned.1.call-start = ((), (), s32[]{:S(2)}) async-start(), calls=%async_computation.6 | async-start | bytes 2621440 | tf_op jit(solution)/shard_map/all_gather | solution.py:177
  303.7 1.2 copy-start.10
  303.7 1.2 copy-start.13
  354.6 1.4 copy-start.2
  356.0 3.9 %copy-start.11 = (f32[2048]{0:T(1024)S(1)}, f32[2048]{0:T(1024)}, u32[]{:S(2)}) copy-start(f32[2048]{0:T(1024)} %param.30) | copy-start | bytes 24580
  356.0 5.0 %copy-start.1 = (bf16[1,512,2048]{2,1,0:T(8,128)(2,1)S(1)}, bf16[1,512,2048]{2,1,0:T(8,128)(2,1)}, u32[]{:S(2)}) copy-start(bf16[1,512,2048]{2,1,0:T(8,128)(2,1)} %param.33) | copy-start | bytes 6291460
Sparse Core Ops, SparseCore 0:
  84.1 81.7 all-gather.11
  167.7 41.8 all-gather.5
  211.4 17.5 all-gather.7
  306.3 35.6 all-gather.9
where the time goes:
time: 369 us; the launch traced here: 368 us
  waiting for transfers between devices  145 us (39%)
  blocking collectives  76.4 us (21%)
  other arithmetic  51.6 us (14%)
  matrix products  31.7 us (9%)
  local copies, waits for them, and re-layouts  26.6 us (7%)
  starting transfers between devices  22 us (6%)
  between operations  14.3 us (4%)
    all_to_all x1, blocking collectives, shards(): lax.all_to_all(packed, EP, split_axis=0, concat_axis=0, tiled=True)  63.2 us
    all_to_all x1, waiting for transfers between devices, sum_at_owner(): lax.all_to_all(in_blocks(shard, dim, length), axis, 0, 0, tiled=True)  48.2 us
    all_gather x2, waiting for transfers between devices, all_blocks(): tiles = lax.all_gather(tiles, axes[k], axis=0, tiled=True)  36.8 us
    all_gather x1, waiting for transfers between devices, shards(): lax.all_gather(state_layer_result, 'tp', axis=1, tiled=True)  35.1 us
    add x16, other arithmetic, advance(): return (jnp.exp(decay_log)[..., None] * state + addition, state)  16.4 us
    all_gather x1, waiting for transfers between devices, shards(): lax.all_gather(arrived.reshape(-1, arrived.shape[2]), 'tp', axis=0, tiled...  15.9 us
    all_gather x1, blocking collectives, all_blocks(): tiles = lax.all_gather(tiles, axes[k], axis=0, tiled=True)  13.2 us
    dynamic_update_slice x16, other arithmetic, shards(): lax.scan(advance, jnp.zeros((groups_each_device, HEAD, HEAD), jnp.float32...  10.6 us
  transfers between devices with their start and end apart: 7, of which 6 were waited for; matrix products, arithmetic and copies ran while one was open for 22% of the time, Pallas kernels for 0%

commit v1 on v0

--- a/solution.py
+++ b/solution.py
@@ -35,7 +35,9 @@
 def all_blocks(shard, axes, order):
     tiles = shard[None]
     for k in order:
-        tiles = lax.all_gather(tiles, axes[k], axis=0, tiled=True)
+        tiles = jnp.concatenate(
+            lax.all_to_all(jnp.stack([tiles] * lax.axis_size(axes[k])), axes[k], 0, 0), axis=0
+        )
     current = [lax.axis_size(axes[k]) for k in reversed(order)]
     tiles = tiles.reshape(*current, *shard.shape)
     turned = sorted(range(len(order)), key=lambda place: order[len(order) - 1 - place])

time: 369 us -> 403 us (1.092)
  waiting for transfers between devices: 145 us -> 164 us
  starting transfers between devices: 22 us -> 34.3 us
  other arithmetic: 51.6 us -> 55.9 us
    all_to_all x1, waiting for transfers between devices: 48.2 us -> 85.3 us  [sum_at_owner(): lax.all_to_all(in_blocks(shard, dim, length), axis, 0, 0, tiled=True)]
    all_gather x2 -> x0, waiting for transfers between devices: 36.8 us -> none  [all_blocks(): tiles = lax.all_gather(tiles, axes[k], axis=0, tiled=True)]
    all_to_all x0 -> x1, waiting for transfers between devices: none -> 35.1 us  [shards(): lax.all_to_all(packed, EP, split_axis=0, concat_axis=0, tiled=True)]
    all_gather x1, waiting for transfers between devices: 15.9 us -> 0.01 us  [shards(): lax.all_gather(arrived.reshape(-1, arrived.shape[2]), 'tp', axis=0, tiled...]
    all_gather x1 -> x0, blocking collectives: 13.2 us -> none  [all_blocks(): tiles = lax.all_gather(tiles, axes[k], axis=0, tiled=True)]
    all_to_all x0 -> x1, starting transfers between devices: none -> 12.4 us  [shards(): lax.all_to_all(packed, EP, split_axis=0, concat_axis=0, tiled=True)]
    all_to_all x1 -> x3, blocking collectives: 63.2 us -> 75 us  [all_blocks(): lax.all_to_all(jnp.stack([tiles] * lax.axis_size(axes[k])), axes[k], 0, 0)]
    another operation x3 -> x4, other arithmetic: 0.7 us -> 5.28 us  [the longest x1 4.58 us: all_blocks(): jnp.stack([tiles] * lax.axis_size(axes[k]))]
  transfers between devices with their start and end apart: 7 -> 6, of which waited for: 6 -> 4; matrix products, arithmetic and copies ran while one was open for 22% -> 21% of each run, Pallas kernels for 0% -> 0%
where the time goes in v1:
time: 403 us; the launch traced here: 402 us
  waiting for transfers between devices  164 us (41%)
  blocking collectives  75 us (19%)
  other arithmetic  55.9 us (14%)
  starting transfers between devices  34.3 us (9%)
  matrix products  31.9 us (8%)
  local copies, waits for them, and re-layouts  25.5 us (6%)
  between operations  14.6 us (4%)
    all_to_all x1, waiting for transfers between devices, sum_at_owner(): lax.all_to_all(in_blocks(shard, dim, length), axis, 0, 0, tiled=True)  85.3 us
    all_to_all x3, blocking collectives, all_blocks(): lax.all_to_all(jnp.stack([tiles] * lax.axis_size(axes[k])), axes[k], 0, 0)  75 us
    all_gather x1, waiting for transfers between devices, shards(): lax.all_gather(state_layer_result, 'tp', axis=1, tiled=True)  35.3 us
    all_to_all x1, waiting for transfers between devices, shards(): lax.all_to_all(packed, EP, split_axis=0, concat_axis=0, tiled=True)  35.1 us
    add x16, other arithmetic, advance(): return (jnp.exp(decay_log)[..., None] * state + addition, state)  16.5 us
    all_to_all x1, starting transfers between devices, shards(): lax.all_to_all(packed, EP, split_axis=0, concat_axis=0, tiled=True)  12.4 us
    dynamic_update_slice x16, other arithmetic, shards(): lax.scan(advance, jnp.zeros((groups_each_device, HEAD, HEAD), jnp.float32...  10.6 us
    all_to_all x1, starting transfers between devices, shards(): lax.all_to_all(finished, EP, split_axis=0, concat_axis=0, tiled=True)  10.4 us
  transfers between devices with their start and end apart: 6, of which 4 were waited for; matrix products, arithmetic and copies ran while one was open for 21% of the time, Pallas kernels for 0%

profile of v1, /device:TPU:8, one launch (start us, length us, event | category | flops | bytes accessed | tf_op | source)
XLA Modules:
  0.0 401.5 jit_solution(9616802578044558012)
XLA Ops:
  9.9 1.4 scatter_custom_fusion.1
  11.4 1.2 fusion.17
  12.6 1.5 scatter_custom_fusion
  14.2 1.3 fusion.19
  15.5 3.3 gather_fusion
  18.8 3.1 bitcast_select_fusion
  21.9 12.4 %all-to-all-start.4 = ((bf16[64,8,2048]{2,1,0:T(8,128)(2,1)}), bf16[64,8,2048]{2,1,0:T(8,128)(2,1)}, u32[]{:S(2)}, u32[]{:S(2)}) async-start(bf16[64,8,2048]{2,1,0:T(8,128)(2,1)} %bitcast_select_fusion), calls=%async_computation.4 | async-start | bytes 4194304 | tf_op jit(solution)/shard_map/all_to_all | solution.py:195
  34.5 1.3 divide_multiply_fusion
  35.7 1.7 reshape.259
  37.6 2.3 fusion.12
  39.9 2.7 reshape.258
  42.7 2.0 reshape.261
  45.9 2.7 bitcast_multiply_fusion.5
  48.5 1.9 fusion.25
  50.4 35.1 %all-to-all-done.4 = bf16[64,8,2048]{2,1,0:T(8,128)(2,1)} async-done(((bf16[64,8,2048]{2,1,0:T(8,128)(2,1)}), bf16[64,8,2048]{2,1,0:T(8,128)(2,1)}, u32[]{:S(2)}, u32[]{:S(2)}) %all-to-all-start.4) | async-done | bytes 2097184 | tf_op jit(solution)/shard_map/all_to_all | solution.py:195
  85.5 27.6 %while.13 = (s32[]{:T(128)}, f32[2,128,128]{2,1,0:T(8,128)S(1)}, f32[16,2,128,128]{3,2,1,0:T(8,128)}, f32[16,2,128]{2,1,0:T(2,128)S(1)}, f32[16,2,128,128]{3,2,1,0:T(8,128)}, /*index=5*/s32[]{:T(128)}, s32[]{:T(128)}) while((s32[]{:T(128)}, f32[2,128,128]{2,1,0:T(8,128)S(1)}, f32[16,2,128,128]{3,2,1,0:T(8,128)}, ...), condition=%wide.region_2.3_spmd.clone, body=%wide.region_1.2_spmd.clone.sunk | while | flops 131075 | bytes 659040 | solution.py:149
  91.3 1.0 bitcast_add_fusion.2
  93.1 1.0 bitcast_add_fusion.2
  94.8 1.1 bitcast_add_fusion.2
  96.6 1.0 bitcast_add_fusion.2
  98.3 1.0 bitcast_add_fusion.2
  100.0 1.0 bitcast_add_fusion.2
  105.2 1.0 bitcast_add_fusion.2
  106.9 1.0 bitcast_add_fusion.2
  108.7 1.0 bitcast_add_fusion.2
  112.1 1.0 bitcast_add_fusion.2
  113.2 9.8 %all_to_all.35 = bf16[4,1,1,2,128,128]{5,4,3,2,1,0:T(8,128)(2,1)S(1)} all-to-all(bf16[4,1,1,2,128,128]{5,4,3,2,1,0:T(8,128)(2,1)S(1)} %stack.9), channel_id=1, replica_groups=mesh['ep_0'=8,'ep_1'=4,'ep_2'=2,'tp'=4] {'ep_1'}, dimensions={0} | all-to-all | bytes 524288 | tf_op jit(solution)/shard_map/all_to_all | solution.py:39
  123.5 53.4 %all_to_all.36 = bf16[8,4,1,2,128,128]{5,4,3,1,2,0:T(8,128)(2,1)} all-to-all(bf16[8,4,1,2,128,128]{5,4,3,1,2,0:T(8,128)(2,1)S(1)} %stack.10), channel_id=1, replica_groups=mesh['ep_0'=8,'ep_1'=4,'ep_2'=2,'tp'=4] {'ep_0'}, dimensions={0} | all-to-all | bytes 4194304 | tf_op jit(solution)/shard_map/all_to_all | solution.py:39
  177.5 5.3 %all-to-all-start = ((f32[64,1,2,128]{3,2,1,0:T(2,128)}), f32[64,1,2,128]{3,2,1,0:T(2,128)S(1)}, u32[]{:S(2)}, u32[]{:S(2)}) async-start(f32[64,1,2,128]{3,2,1,0:T(2,128)} %broadcast_in_dim.52), calls=%async_computation | async-start | bytes 131072 | tf_op jit(solution)/shard_map/all_to_all | solution.py:19
  182.8 4.6 %pad_maximum_fusion = bf16[2,32,1,2,128,128]{5,4,3,1,2,0:T(8,128)(2,1)} fusion(bf16[1,32,1,2,128,128]{5,4,3,1,2,0:T(8,128)(2,1)} %bitcast.107), kind=kLoop, calls=%fused_computation.9 | loop fusion | flops 2097152 | bytes 6291456 | tf_op jit(solution)/shard_map/stack | solution.py:39
  187.4 7.7 %fusion.4 = f32[2048,512]{1,0:T(8,128)S(1)} fusion(bf16[2048,2048]{1,0:T(8,128)(2,1)} %all-gather.5.cloned.1.call-done, bf16[1,2048,512]{2,1,0:T(8,128)(2,1)} %param.31), kind=kOutput, calls=%fused_computation.15 | convolution fusion | flops 4294967296 | bytes 14680064 | tf_op jit(solution)/shard_map/dot_general | solution.py:197
  195.1 5.6 %multiply_convert_fusion = bf16[2048,512]{1,0:T(8,128)(2,1)S(1)} fusion(f32[2048,512]{1,0:T(8,128)S(1)} %fusion.4, bf16[2048,2048]{1,0:T(8,128)(2,1)S(1)} %copy-done.15, bf16[1,2048,512]{2,1,0:T(8,128)(2,1)S(1)} %copy-done.16), kind=kOutput, calls=%fused_computation.12 | convolution fusion | flops 4305453056 | bytes 16777216 | tf_op jit(solution)/shard_map/dot_general | solution.py:198
  200.7 6.8 %convolution_convert_fusion = bf16[2048,2048]{1,0:T(8,128)(2,1)} fusion(bf16[2048,512]{1,0:T(8,128)(2,1)S(1)} %multiply_convert_fusion, bf16[1,512,2048]{2,1,0:T(8,128)(2,1)S(1)} %copy-done), kind=kOutput, calls=%fused_computation.8 | convolution fusion | flops 4299161600 | bytes 12582912 | tf_op jit(solution)/shard_map/dot_general | solution.py:201
  207.5 11.8 %all_to_all.37 = bf16[2,32,1,2,128,128]{5,4,3,1,2,0:T(8,128)(2,1)} all-to-all(bf16[2,32,1,2,128,128]{5,4,3,1,2,0:T(8,128)(2,1)} %pad_maximum_fusion), channel_id=1, replica_groups=mesh['ep_0'=8,'ep_1'=4,'ep_2'=2,'tp'=4] {'ep_2'}, dimensions={0} | all-to-all | bytes 8388608 | tf_op jit(solution)/shard_map/all_to_all | solution.py:39
  219.4 5.9 %all-to-all-start.5 = ((bf16[4,512,2048]{2,1,0:T(8,128)(2,1)}), bf16[4,512,2048]{2,1,0:T(8,128)(2,1)}, u32[]{:S(2)}, u32[]{:S(2)}) async-start(bf16[4,512,2048]{2,1,0:T(8,128)(2,1)} %bitcast.108), calls=%async_computation.5 | async-start | bytes 16777216 | tf_op jit(solution)/shard_map/all_to_all | solution.py:58
  225.7 2.5 copy.61
  228.3 2.8 fusion
  231.1 1.1 fusion.6
  232.3 1.9 multiply_reduce_fusion.1
  234.2 85.3 %all-to-all-done.5 = bf16[4,512,2048]{2,1,0:T(8,128)(2,1)} async-done(((bf16[4,512,2048]{2,1,0:T(8,128)(2,1)}), bf16[4,512,2048]{2,1,0:T(8,128)(2,1)}, u32[]{:S(2)}, u32[]{:S(2)}) %all-to-all-start.5) | async-done | bytes 8388640 | tf_op jit(solution)/shard_map/all_to_all | solution.py:58
  319.4 7.2 %reduce_sum.70 = bf16[512,2048]{1,0:T(8,128)(2,1)} reduce(bf16[4,512,2048]{2,1,0:T(8,128)(2,1)} %all-to-all-done.5, bf16[]{:T(256)} %constant.117.clone.1), dimensions={0}, to_apply=%region_13.14 | reduce | flops 3145728 | bytes 10485762 | tf_op jit(solution)/shard_map/reduce_sum | solution.py:59
  326.7 10.4 %all-to-all-start.6 = ((bf16[64,8,2048]{2,1,0:T(8,128)(2,1)}), bf16[64,8,2048]{2,1,0:T(8,128)(2,1)S(1)}, u32[]{:S(2)}, u32[]{:S(2)}) async-start(bf16[64,8,2048]{2,1,0:T(8,128)(2,1)} %bitcast.109), calls=%async_computation.6 | async-start | bytes 4194304 | tf_op jit(solution)/shard_map/all_to_all | solution.py:208
  338.6 1.1 fusion.33
  340.7 35.3 %all-gather.3.cloned.1.call-done = bf16[1024,1024]{1,0:T(8,128)(2,1)} async-done(((bf16[1024,256]{1,0:T(8,128)(2,1)}), bf16[1024,1024]{1,0:T(8,128)(2,1)}) %all-gather.3.cloned.1.call-update) | async-done | bytes 2097168 | tf_op jit(solution)/shard_map/all_gather | solution.py:179
  376.0 4.1 %convolution_convert_fusion.1 = bf16[1024,512]{1,0:T(8,128)(2,1)} fusion(bf16[1024,1024]{1,0:T(8,128)(2,1)} %all-gather.3.cloned.1.call-done, bf16[1024,512]{1,0:T(8,128)(2,1)} %param.25), kind=kOutput, calls=%fused_computation.21 | convolution fusion | flops 1074266112 | bytes 4194304 | tf_op jit(solution)/shard_map/dot_general | solution.py:178
  380.1 8.2 %all-to-all-done.6 = bf16[64,8,2048]{2,1,0:T(8,128)(2,1)S(1)} async-done(((bf16[64,8,2048]{2,1,0:T(8,128)(2,1)}), bf16[64,8,2048]{2,1,0:T(8,128)(2,1)S(1)}, u32[]{:S(2)}, u32[]{:S(2)}) %all-to-all-start.6) | async-done | bytes 2097184 | tf_op jit(solution)/shard_map/all_to_all | solution.py:208
  389.7 3.5 gather_fusion.2
  393.5 1.1 multiply_convert_fusion.1
  (131 shorter events, 26.9 us)
Async XLA Ops:
  7.2 193.6 %copy-start = (bf16[1,512,2048]{2,1,0:T(8,128)(2,1)S(1)}, bf16[1,512,2048]{2,1,0:T(8,128)(2,1)}, u32[]{:S(2)}) copy-start(bf16[1,512,2048]{2,1,0:T(8,128)(2,1)} %param.33) | copy-start | bytes 6291460
  21.9 12.5 %copy-start.9 = (bf16[1024,256]{1,0:T(8,128)(2,1)S(1)}, bf16[1024,256]{1,0:T(8,128)(2,1)}, u32[]{:S(2)}) copy-start(bf16[1024,256]{1,0:T(8,128)(2,1)} %param.19) | copy-start | bytes 1572868
  21.9 12.5 %copy-start.14 = (f32[256]{0:T(256)S(1)}, f32[256]{0:T(256)}, u32[]{:S(2)}) copy-start(f32[256]{0:T(256)} %param.22) | copy-start | bytes 3076
  21.9 63.6 %all-to-all-start.4 = ((bf16[64,8,2048]{2,1,0:T(8,128)(2,1)}), bf16[64,8,2048]{2,1,0:T(8,128)(2,1)}, u32[]{:S(2)}, u32[]{:S(2)}) async-start(bf16[64,8,2048]{2,1,0:T(8,128)(2,1)} %bitcast_select_fusion), calls=%async_computation.4 | async-start | bytes 4194304 | tf_op jit(solution)/shard_map/all_to_all | solution.py:195
  34.4 3.1 copy-start.12
  34.4 153.0 %all-gather.5.cloned.1.call-start = ((), (), s32[]{:S(2)}) async-start(), calls=%async_computation.8 | async-start | bytes 10485760 | tf_op jit(solution)/shard_map/all_gather | solution.py:196
  44.6 1.2 copy-start.5
  45.9 2.7 copy-start.3
  177.5 30.0 %all-to-all-start = ((f32[64,1,2,128]{3,2,1,0:T(2,128)}), f32[64,1,2,128]{3,2,1,0:T(2,128)S(1)}, u32[]{:S(2)}, u32[]{:S(2)}) async-start(f32[64,1,2,128]{3,2,1,0:T(2,128)} %broadcast_in_dim.52), calls=%async_computation | async-start | bytes 131072 | tf_op jit(solution)/shard_map/all_to_all | solution.py:19
  187.4 7.7 %copy-start.15 = (bf16[2048,2048]{1,0:T(8,128)(2,1)S(1)}, bf16[2048,2048]{1,0:T(8,128)(2,1)}, u32[]{:S(2)}) copy-start(bf16[2048,2048]{1,0:T(8,128)(2,1)} %all-gather.5.cloned.1.call-done) | copy-start | bytes 25165828
  187.4 7.7 %copy-start.16 = (bf16[1,2048,512]{2,1,0:T(8,128)(2,1)S(1)}, bf16[1,2048,512]{2,1,0:T(8,128)(2,1)}, u32[]{:S(2)}) copy-start(bf16[1,2048,512]{2,1,0:T(8,128)(2,1)} %param.32) | copy-start | bytes 6291460
  219.4 100.1 %all-to-all-start.5 = ((bf16[4,512,2048]{2,1,0:T(8,128)(2,1)}), bf16[4,512,2048]{2,1,0:T(8,128)(2,1)}, u32[]{:S(2)}, u32[]{:S(2)}) async-start(bf16[4,512,2048]{2,1,0:T(8,128)(2,1)} %bitcast.108), calls=%async_computation.5 | async-start | bytes 16777216 | tf_op jit(solution)/shard_map/all_to_all | solution.py:58
  228.2 2.9 copy-start.7
  228.2 2.9 copy-start.8
  231.1 1.1 copy-start.4
  231.1 1.2 copy-start.6
  326.7 61.7 %all-to-all-start.6 = ((bf16[64,8,2048]{2,1,0:T(8,128)(2,1)}), bf16[64,8,2048]{2,1,0:T(8,128)(2,1)S(1)}, u32[]{:S(2)}, u32[]{:S(2)}) async-start(bf16[64,8,2048]{2,1,0:T(8,128)(2,1)} %bitcast.109), calls=%async_computation.6 | async-start | bytes 4194304 | tf_op jit(solution)/shard_map/all_to_all | solution.py:208
  337.1 38.9 %all-gather.3.cloned.1.call-start = ((), (), s32[]{:S(2)}) async-start(), calls=%async_computation.7 | async-start | bytes 2621440 | tf_op jit(solution)/shard_map/all_gather | solution.py:179
  337.4 1.2 copy-start.10
  337.4 1.2 copy-start.13
  388.3 1.4 copy-start.2
  389.7 3.9 copy-start.11
  389.7 5.0 %copy-start.1 = (bf16[1,512,2048]{2,1,0:T(8,128)(2,1)S(1)}, bf16[1,512,2048]{2,1,0:T(8,128)(2,1)}, u32[]{:S(2)}) copy-start(bf16[1,512,2048]{2,1,0:T(8,128)(2,1)} %param.33) | copy-start | bytes 6291460
Sparse Core Ops, SparseCore 0:
  85.7 81.7 all-gather.4
  340.3 35.6 all-gather.2
